TPU v7x, 32 devices: a whole 2x2x4 slice. The times are simulated.
32 devices in a mesh: sp: 4 (over y, x), dp: 8 (over z, core).
Axes of the slice: x: 2, y: 2, z: 4, core: 2. Of those that a mesh axis runs over, the one named last changes fastest.
Arguments:
- tokens: bfloat16 [8, 1024, 2048], P('dp', 'sp'), may hold values from -6 to 6
- in_gain: float32 [2048], replicated, may hold values from 0.1 to 1.9
- query_weight: bfloat16 [2048, 2048], P('dp'), may hold values from -1 to 1
- key_weight: bfloat16 [2048, 512], P('dp'), may hold values from -1 to 1
- value_matrix: bfloat16 [2048, 512], P('dp'), may hold values from -0.125 to 0.125
- query_gain: float32 [128], replicated, may hold values from 1 to 6
- key_gain: float32 [128], replicated, may hold values from 1 to 6
- out_weight: bfloat16 [2048, 2048], P('dp'), may hold values from -0.125 to 0.125
- out_gain: float32 [2048], replicated, may hold values from 0.1 to 1.9
Outputs:
- mixed: bfloat16 [8, 1024, 2048], P('dp', 'sp')
All inputs are finite; a program needn't handle non-finite values.
Results may differ from a plain program's by a relative error of at most 0.0055.
The roundings to bfloat16 on the way count: a program that leaves them out, or rounds other values in their place, can miss the bound.
Values may be sent and summed in bfloat16 or wider, within the bound.
A program may use at most 128 MiB of HBM per device.

v0:
```python
import jax
import jax.numpy as jnp
from jax import lax
from jax.sharding import PartitionSpec as P

QUERY_HEAD_COUNT = 16
KEY_VALUE_HEADS = 4
HEAD_WIDTH = 128
GRID_W = 64


EPS = 1e-06
THETA = 10000.0


def norm_rows(row_data, gain_vec):
    return (
        row_data * lax.rsqrt(jnp.mean(row_data * row_data, axis=-1, keepdims=True) + EPS) * gain_vec
    )


def rotate(head_data, positions):
    head_size = head_data.shape[-1]
    half_size = head_size // 2
    quarter = head_size // 4
    inverse_freq = THETA ** (-jnp.arange(quarter, dtype=jnp.float32) / quarter)
    row_angle = (positions // GRID_W).astype(jnp.float32)[:, None] * inverse_freq[None, :]
    col_angle = (positions % GRID_W).astype(jnp.float32)[:, None] * inverse_freq[None, :]

    def turn_half(half_part, angle):
        cosine = jnp.cos(angle)[:, None, :]
        sine_val = jnp.sin(angle)[:, None, :]
        first_part = half_part[..., :quarter]
        second_part = half_part[..., quarter:]
        return jnp.concatenate(
            [
                first_part * cosine - second_part * sine_val,
                second_part * cosine + first_part * sine_val,
            ],
            axis=-1,
        )

    return jnp.concatenate(
        [
            turn_half(head_data[..., :half_size], row_angle),
            turn_half(head_data[..., half_size:], col_angle),
        ],
        axis=-1,
    )


def finish(projected, gain_vec, positions):
    row_count = projected.shape[0]
    heads_data = projected.reshape(row_count, -1, HEAD_WIDTH)
    heads_data = rotate(norm_rows(heads_data, gain_vec), positions)
    return heads_data.reshape(row_count, -1).astype(jnp.bfloat16)


def attend(local_q, local_k, local_v, heads_local, key_value_slice):
    length = local_q.shape[0]
    group_local = heads_local // key_value_slice
    rows_per_block = min(512, length)
    query_block_list = local_q.reshape(
        length // rows_per_block, rows_per_block, key_value_slice, group_local, HEAD_WIDTH
    )
    key_heads = local_k.reshape(length, key_value_slice, HEAD_WIDTH)
    value_heads = local_v.reshape(length, key_value_slice, HEAD_WIDTH)

    def one_block(query_block):
        scores = jnp.einsum(
            "qegd,ked->egqk", query_block, key_heads, preferred_element_type=jnp.float32
        ) * HEAD_WIDTH ** (-0.5)
        shifted = scores - jnp.max(scores, axis=-1, keepdims=True)
        raised = jnp.exp(shifted)
        weights = (raised / jnp.sum(raised, axis=-1, keepdims=True)).astype(jnp.bfloat16)
        attended = jnp.einsum(
            "egqk,ked->qegd", weights, value_heads, preferred_element_type=jnp.float32
        )
        return attended.astype(jnp.bfloat16)

    return lax.map(one_block, query_block_list).reshape(length, heads_local * HEAD_WIDTH)


def on_device(
    tokens,
    in_gain,
    query_weight,
    key_weight,
    value_matrix,
    query_gain,
    key_gain,
    out_weight,
    out_gain,
):
    sequence = tokens[0]
    repeat_heads = lax.axis_size("sp")
    sp_rank = lax.axis_index("sp")
    heads_local = QUERY_HEAD_COUNT // repeat_heads
    key_value_slice = max(1, KEY_VALUE_HEADS // repeat_heads)
    queries_per_group = QUERY_HEAD_COUNT // KEY_VALUE_HEADS
    first_kv = sp_rank * heads_local // queries_per_group
    normed = norm_rows(sequence.astype(jnp.float32), in_gain).astype(jnp.bfloat16)
    q_cols = lax.dynamic_slice_in_dim(
        query_weight, sp_rank * heads_local * HEAD_WIDTH, heads_local * HEAD_WIDTH, 1
    )
    k_cols = lax.dynamic_slice_in_dim(
        key_weight, first_kv * HEAD_WIDTH, key_value_slice * HEAD_WIDTH, 1
    )
    v_cols = lax.dynamic_slice_in_dim(
        value_matrix, first_kv * HEAD_WIDTH, key_value_slice * HEAD_WIDTH, 1
    )
    full_q, full_k, full_v = (
        lax.all_gather(q_cols, "dp", axis=0, tiled=True),
        lax.all_gather(k_cols, "dp", axis=0, tiled=True),
        lax.all_gather(v_cols, "dp", axis=0, tiled=True),
    )
    joined = jnp.concatenate([full_q, full_k, full_v], axis=1)
    query_end = heads_local * HEAD_WIDTH
    key_end = query_end + key_value_slice * HEAD_WIDTH
    shard_rows = lax.all_gather(normed, "sp", axis=0, tiled=True)
    row_count = shard_rows.shape[0]
    blended = jnp.dot(shard_rows, joined, preferred_element_type=jnp.float32)
    positions = jnp.arange(row_count, dtype=jnp.int32)
    part_q = finish(blended[:, :query_end], query_gain, positions)
    part_k = finish(blended[:, query_end:key_end], key_gain, positions)
    part_v = blended[:, key_end:].astype(jnp.bfloat16)
    merged = jnp.concatenate([part_q, part_k, part_v], axis=1)
    local_q = merged[:, :query_end]
    local_k = merged[:, query_end:key_end]
    local_v = merged[:, key_end:]
    attended = attend(local_q, local_k, local_v, heads_local, key_value_slice)
    returned = lax.all_to_all(attended, "sp", split_axis=0, concat_axis=1, tiled=True)
    projected = jnp.dot(
        returned,
        lax.all_gather(out_weight, "dp", axis=0, tiled=True),
        preferred_element_type=jnp.float32,
    )
    result = norm_rows(projected, out_gain).astype(jnp.bfloat16)
    return result[None]


def solution(mesh):
    placed = (
        P("dp", "sp", None),
        P(),
        P("dp", None),
        P("dp", None),
        P("dp", None),
        P(),
        P(),
        P("dp", None),
        P(),
    )
    return jax.shard_map(
        on_device, mesh=mesh, in_specs=placed, out_specs=P("dp", "sp", None), check_vma=False
    )
```

profile of v0, /device:TPU:0, one launch (start us, length us, event | category | flops | bytes accessed | tf_op | source)
XLA Modules:
  0.0 197.9 jit_solution(16004750652019674749)
XLA Ops:
  6.5 1.2 copy-done
  7.8 0.7 constant_dynamic-slice_fusion.2
  8.5 0.0 all-gather.6.cloned.1.call-update
  8.5 0.0 all-gather.4.cloned.1.call-start
  8.6 1.5 fusion.24
  10.1 2.0 fusion.26
  12.1 0.0 all-gather.8.cloned.1.call-start
  12.1 0.7 all-gather.8.cloned.1.call-update
  12.9 0.9 constant_dynamic-slice_fusion.1
  13.7 0.8 constant_dynamic-slice_fusion
  14.6 19.1 %all_gather.17 = bf16[2048,128]{1,0:T(8,128)(2,1)S(1)} all-gather(bf16[256,128]{1,0:T(8,128)(2,1)S(1)} %constant_dynamic-slice_fusion.1), channel_id=1, replica_groups=mesh['sp'=4,'dp'=8] {'dp'}, dimensions={0}, use_global_device_ids=true | all-gather | bytes 589824 | tf_op jit(solution)/shard_map/all_gather | solution.py:114
  33.7 16.6 %all_gather.18 = bf16[2048,128]{1,0:T(8,128)(2,1)S(1)} all-gather(bf16[256,128]{1,0:T(8,128)(2,1)S(1)} %constant_dynamic-slice_fusion), channel_id=1, replica_groups=mesh['sp'=4,'dp'=8] {'dp'}, dimensions={0}, use_global_device_ids=true | all-gather | bytes 589824 | tf_op jit(solution)/shard_map/all_gather | solution.py:115
  50.4 5.4 %multiply_cosine_fusion.1 = (f32[1024,32]{1,0:T(8,128)}, f32[1024,32]{1,0:T(8,128)}, f32[1024,32]{1,0:T(8,128)}, f32[1024,32]{1,0:T(8,128)}) fusion(f32[32]{0:T(128)S(1)} %multiply_power_fusion, f32[1024]{0:T(1024)S(1)} %get-tuple-element.75, f32[1024]{0:T(1024)S(1)} %get-tuple-element.76), kind=kLoop, calls=%fused_computation.42 | loop fusion | flops 65536 | bytes 532608 | tf_op jit(solution)/shard_map/cos | solution.py:31
  55.7 44.9 %all-gather.4.cloned.1.call-done = bf16[1024,2048]{1,0:T(8,128)(2,1)} async-done(((bf16[256,2048]{1,0:T(8,128)(2,1)}), bf16[1024,2048]{1,0:T(8,128)(2,1)}) %all-gather.4.cloned.1.call-update) | async-done | bytes 4194320 | tf_op jit(solution)/shard_map/all_gather | solution.py:120
  100.6 6.5 %fusion.18 = f32[1024,768]{0,1:T(8,128)S(1)} fusion(bf16[1024,2048]{1,0:T(8,128)(2,1)} %all-gather.4.cloned.1.call-done, bf16[2048,128]{1,0:T(8,128)(2,1)S(1)} %all_gather.18, bf16[2048,128]{1,0:T(8,128)(2,1)S(1)} %all_gather.17, bf16[2048,512]{1,0:T(8,128)(2,1)} %all-gather.6.cloned.1.call-done), kind=kOutput, calls=%fused_computation.18 | convolution fusion | flops 3230662656 | bytes 10485760 | tf_op jit(solution)/shard_map/dot_general | solution.py:122
  107.1 0.1 slice.57
  107.2 0.1 multiply_reduce_fusion.2
  107.3 1.5 copy-done.1
  108.8 0.1 multiply_bitcast_fusion
  108.9 1.2 fusion.42
  110.1 0.7 pad_maximum_fusion.1
  110.8 1.1 copy.14
  111.9 1.9 copy.12
  113.8 1.9 fusion.28
  115.8 1.8 copy.15
  117.6 1.8 multiply_reduce_fusion.1
  119.5 0.7 multiply_multiply_fusion
  120.2 0.3 copy-done.4
  120.5 0.2 copy-done.5
  120.6 0.2 copy-done.6
  120.8 0.2 copy-done.7
  121.0 1.8 subtract_convert_fusion.1
  122.8 1.3 pad_maximum_fusion
  124.1 11.5 %while.10 = (s32[]{:T(128)}, bf16[2,512,1,4,128]{4,3,1,0,2:T(4,128)(2,1)S(1)}, bf16[2,512,1,4,128]{4,1,0,3,2:T(8,128)(2,1)S(1)}, bf16[1024,1,128]{2,0,1:T(8,128)...) while((s32[]{:T(128)}, bf16[2,512,1,4,128]{4,3,1,0,2:T(4,128)(2,1)S(1)}, ...), condition=%wide.region_6.7_spmd, body=%wide.region_3.6_spmd.sunk | while | flops 1092874240 | bytes 28876904 | solution.py:81
  124.3 1.3 bitcast_reduce_fusion.2
  125.7 1.8 fusion.64
  127.4 2.0 %fusion.65 = bf16[1,512,1,4,128]{4,1,3,2,0:T(8,128)(2,1)S(1)} fusion(f32[4,512]{1,0:T(4,128)S(1)} %fusion.64, f32[4,512]{1,0:T(4,128)S(1)} %get-tuple-element.111, f32[512,4,1024]{2,0,1:T(8,128)S(1)} %get-tuple-element.110, bf16[1024,1,128]{2,0,1:T(8,128)(2,1)S(1)} %copy-done.9), kind=kOutput, calls=%fused_computation.9.clone.1 | convolution fusion | flops 545521664 | bytes 9191424 | tf_op jit(solution)/shard_map/while/body/eval_jaxpr/egqk,ked->qegd/dot_general | solution.py:76
  129.5 0.4 copy_dynamic-update-slice_fusion.2
  130.0 1.3 bitcast_reduce_fusion.2
  131.3 1.8 fusion.64
  133.1 2.0 %fusion.65 = bf16[1,512,1,4,128]{4,1,3,2,0:T(8,128)(2,1)S(1)} fusion(f32[4,512]{1,0:T(4,128)S(1)} %fusion.64, f32[4,512]{1,0:T(4,128)S(1)} %get-tuple-element.111, f32[512,4,1024]{2,0,1:T(8,128)S(1)} %get-tuple-element.110, bf16[1024,1,128]{2,0,1:T(8,128)(2,1)S(1)} %copy-done.9), kind=kOutput, calls=%fused_computation.9.clone.1 | convolution fusion | flops 545521664 | bytes 9191424 | tf_op jit(solution)/shard_map/while/body/eval_jaxpr/egqk,ked->qegd/dot_general | solution.py:76
  135.1 0.4 copy_dynamic-update-slice_fusion.2
  135.6 0.4 all_to_all.14
  136.1 16.7 %all_to_all.19 = bf16[4,256,512]{2,1,0:T(8,128)(2,1)S(1)} all-to-all(bf16[4,256,512]{2,1,0:T(8,128)(2,1)S(1)} %all_to_all.14), channel_id=1, replica_groups=mesh['sp'=4,'dp'=8] {'sp'}, dimensions={0} | all-to-all | bytes 2097152 | tf_op jit(solution)/shard_map/all_to_all | solution.py:132
  152.7 0.5 copy.17
  153.3 31.0 %all-gather.8.cloned.1.call-done = bf16[2048,2048]{1,0:T(8,128)(2,1)} async-done(((bf16[256,2048]{1,0:T(8,128)(2,1)}), bf16[2048,2048]{1,0:T(8,128)(2,1)}) %all-gather.8.cloned.1.call-update) | async-done | bytes 8388624 | tf_op jit(solution)/shard_map/all_gather | solution.py:135
  184.3 5.8 %multiply_reduce_fusion = (f32[256]{0:T(256)S(1)}, f32[256,2048]{1,0:T(8,128)S(1)}) fusion(bf16[256,2048]{0,1:T(8,128)(2,1)S(1)} %bitcast.90, bf16[2048,2048]{1,0:T(8,128)(2,1)} %all-gather.8.cloned.1.call-done), kind=kOutput, calls=%fused_computation.30 | convolution fusion | flops 2148531968 | bytes 11535360 | tf_op jit(solution)/shard_map/dot_general | solution.py:133
  190.1 1.2 fusion.27
  (32 shorter events, 0.1 us)
Async XLA Ops:
  6.5 1.2 copy-start
  6.5 3.6 %copy-start.3 = (bf16[1,256,2048]{2,1,0:T(8,128)(2,1)S(1)}, bf16[1,256,2048]{2,1,0:T(8,128)(2,1)}, u32[]{:S(2)}) copy-start(bf16[1,256,2048]{2,1,0:T(8,128)(2,1)} %param.11) | copy-start | bytes 3145732
  6.5 49.2 %all-gather.6.cloned.1.call-start = ((), (), s32[]{:S(2)}) async-start(), calls=%async_computation.2 | async-start | bytes 2359296 | tf_op jit(solution)/shard_map/all_gather | solution.py:113
  8.5 92.1 %all-gather.4.cloned.1.call-start = ((), (), s32[]{:S(2)}) async-start(), calls=%async_computation.1 | async-start | bytes 5242880 | tf_op jit(solution)/shard_map/all_gather | solution.py:120
  12.1 172.2 %all-gather.8.cloned.1.call-start = ((), (), s32[]{:S(2)}) async-start(), calls=%async_computation.3 | async-start | bytes 9437184 | tf_op jit(solution)/shard_map/all_gather | solution.py:135
  107.1 1.7 copy-start.1
  107.1 1.7 copy-start.11
  113.8 5.6 %copy-start.2 = (f32[1024,4,128]{2,0,1:T(8,128)S(1)}, f32[1024,4,128]{2,0,1:T(8,128)}, u32[]{:S(2)}) copy-start(f32[1024,4,128]{2,0,1:T(8,128)} %copy.12) | copy-start | bytes 6291460
  113.8 5.6 %copy-start.12 = (f32[128]{0:T(128)S(1)}, f32[128]{0:T(128)}, u32[]{:S(2)}) copy-start(f32[128]{0:T(128)} %param.16) | copy-start | bytes 1540
  119.4 1.0 copy-start.4
  119.5 1.2 copy-start.5
  119.5 1.3 copy-start.6
  119.5 1.5 copy-start.7
  122.8 1.4 copy-start.8
  125.7 1.8 copy-start.9
  131.3 1.8 copy-start.9
  184.3 5.8 %copy-start.10 = (f32[2048]{0:T(1024)S(1)}, f32[2048]{0:T(1024)}, u32[]{:S(2)}) copy-start(f32[2048]{0:T(1024)} %param.19) | copy-start | bytes 24580
Sparse Core Ops, SparseCore 0:
  8.9 37.4 all-gather.5
  48.2 52.3 all-gather.3
  102.2 82.0 all-gather.7
where the time goes:
time: 198 us
  waiting for transfers between devices  76.6 us (39%)
  blocking collectives  52.4 us (26%)
  other arithmetic  21.4 us (11%)
  matrix products  19 us (10%)
  local copies, waits for them, and re-layouts  14.7 us (7%)
  between operations  13.4 us (7%)
    all_gather x1, waiting for transfers between devices, on_device(): shard_rows = lax.all_gather(normed, 'sp', axis=0, tiled=True)  44.9 us
    all_gather x1, waiting for transfers between devices, on_device(): lax.all_gather(out_weight, 'dp', axis=0, tiled=True)  31 us
    all_gather x1, blocking collectives, on_device(): lax.all_gather(k_cols, 'dp', axis=0, tiled=True)  19.1 us
    all_to_all x1, blocking collectives, on_device(): lax.all_to_all(attended, 'sp', split_axis=0, concat_axis=1, tiled=True)  16.7 us
    all_gather x1, blocking collectives, on_device(): lax.all_gather(v_cols, 'dp', axis=0, tiled=True)  16.6 us
    dot_general x1, matrix products, on_device(): blended = jnp.dot(shard_rows, joined, preferred_element_type=jnp.float32)  6.45 us
    dot_general x1, matrix products, on_device(): jnp.dot(returned, lax.all_gather(out_weight, 'dp', axis=0, tiled=True), p...  5.82 us
    cos x1, other arithmetic, turn_half(): cosine = jnp.cos(angle)[:, None, :]  5.36 us
  transfers between devices with their start and end apart: 3, of which 2 were waited for; matrix products, arithmetic and copies ran while one was open for 22% of the time, Pallas kernels for 0%

commit v1 on v0

v1 whole, which is shorter than its diff:
```python
import functools

import jax
import jax.numpy as jnp
import numpy as np
from jax import lax
from jax.experimental import pallas as pl
from jax.experimental.pallas import tpu as pltpu
from jax.sharding import PartitionSpec as P

QUERY_HEAD_COUNT = 16
KEY_VALUE_HEADS = 4
HEAD_WIDTH = 128
GRID_W = 64
EPS = 1e-06
THETA = 10000.0
MESH = pl.DeviceIdType.MESH
ANY = pl.BlockSpec(memory_space=pl.ANY)


def remote(src, dst, send_sem, recv_sem, device):
    return pltpu.make_async_remote_copy(
        src_ref=src, dst_ref=dst, send_sem=send_sem, recv_sem=recv_sem,
        device_id=device, device_id_type=MESH,
    )


def gather_kernel(
    parts, chips, q_width, kv_width, first_kv_of,
    x_ref, wq_ref, wk_ref, wv_ref, rows_ref, cols_ref,
    stage, x_send, x_recv, own_sem, stage_sem,
    up_send, up_recv, down_send, down_recv, pair_send, pair_recv,
):
    sp, dp = lax.axis_index("sp"), lax.axis_index("dp")
    z, core = dp // 2, dp % 2
    partner = z * 2 + (1 - core)
    row_count = x_ref.shape[0]
    depth = stage.shape[0]
    square = parts == 4

    first_kv = first_kv_of(sp)
    loads = [
        pltpu.make_async_copy(
            wq_ref.at[:, pl.ds(pl.multiple_of(sp * q_width, 128), q_width)],
            stage.at[:, pl.ds(0, q_width)], stage_sem.at[0]),
        pltpu.make_async_copy(
            wk_ref.at[:, pl.ds(pl.multiple_of(first_kv * HEAD_WIDTH, 128), kv_width)],
            stage.at[:, pl.ds(q_width, kv_width)], stage_sem.at[1]),
        pltpu.make_async_copy(
            wv_ref.at[:, pl.ds(pl.multiple_of(first_kv * HEAD_WIDTH, 128), kv_width)],
            stage.at[:, pl.ds(q_width + kv_width, kv_width)], stage_sem.at[2]),
    ]
    for load in loads:
        load.start()

    barrier = pltpu.get_barrier_semaphore()
    if square:
        x_side = (sp // 2) * 2 + (1 - sp % 2)
        y_side = (1 - sp // 2) * 2 + sp % 2
        corner = (1 - sp // 2) * 2 + (1 - sp % 2)
        greeted = [x_side, y_side]
    else:
        greeted = [lax.rem(sp + i, parts) for i in range(1, parts)]
    for peer in greeted:
        pl.semaphore_signal(barrier, inc=1, device_id={"sp": peer, "dp": dp}, device_id_type=MESH)
    pl.semaphore_signal(barrier, inc=1, device_id={"sp": sp, "dp": partner}, device_id_type=MESH)

    @pl.when(z < chips - 1)
    def _():
        pl.semaphore_signal(barrier, inc=1, device_id={"sp": sp, "dp": dp + 2}, device_id_type=MESH)

    @pl.when(z > 0)
    def _():
        pl.semaphore_signal(barrier, inc=1, device_id={"sp": sp, "dp": dp - 2}, device_id_type=MESH)

    in_chain = (z + chips - 1) // chips + (2 * chips - 2 - z) // chips
    pl.semaphore_wait(barrier, len(greeted) + 1 + in_chain)

    def token_rows(owner, half=None):
        if half is None:
            return rows_ref.at[pl.ds(owner * row_count, row_count)]
        return rows_ref.at[pl.ds(owner * row_count + half * (row_count // 2), row_count // 2)]

    token_sends = []
    if square:
        for half_x, half_y in ((0, 1), (1, 0)):
            for slot, half, peer in ((0, half_x, x_side), (1, half_y, y_side)):
                copy = remote(
                    x_ref.at[pl.ds(half * (row_count // 2), row_count // 2)],
                    token_rows(sp, half), x_send.at[slot * 2 + half],
                    x_recv.at[slot * 2 + half], {"sp": peer, "dp": dp})
                copy.start()
                token_sends.append(copy)
    else:
        for i, peer in enumerate(greeted):
            copy = remote(
                x_ref, token_rows(sp), x_send.at[i], x_recv.at[i], {"sp": peer, "dp": dp})
            copy.start()
            token_sends.append(copy)
    own_rows = pltpu.make_async_copy(x_ref, token_rows(sp), own_sem.at[0])
    own_rows.start()

    for load in loads:
        load.wait()

    def block(owner_z, owner_core):
        return cols_ref.at[pl.ds((owner_z * 2 + owner_core) * depth, depth)]

    def to_up(src, k):
        return remote(src, block(z - k, core), up_send.at[k], up_recv.at[k + 1],
                      {"sp": sp, "dp": dp + 2})

    def to_down(src, k):
        return remote(src, block(z + k, core), down_send.at[k], down_recv.at[k + 1],
                      {"sp": sp, "dp": dp - 2})

    def to_pair(src, owner_z):
        return remote(src, block(owner_z, core), pair_send.at[owner_z], pair_recv.at[owner_z],
                      {"sp": sp, "dp": partner})

    @pl.when(z < chips - 1)
    def _():
        to_up(stage, 0).start()

    @pl.when(z > 0)
    def _():
        to_down(stage, 0).start()

    to_pair(stage, z).start()
    own_cols = pltpu.make_async_copy(stage, block(z, core), own_sem.at[1])
    own_cols.start()

    if square:
        got_x = remote(x_ref.at[pl.ds(0, row_count // 2)], token_rows(x_side, 0),
                       x_send.at[0], x_recv.at[0], {"sp": x_side, "dp": dp})
        got_y = remote(x_ref.at[pl.ds(0, row_count // 2)], token_rows(y_side, 1),
                       x_send.at[3], x_recv.at[3], {"sp": y_side, "dp": dp})

    def relay_columns(k):
        @pl.when(z >= k)
        def _():
            source = block(z - k, core)
            remote(source, source, up_send.at[k], up_recv.at[k], {"sp": sp, "dp": partner}).wait_recv()
            if k < chips - 1:
                @pl.when(z < chips - 1)
                def _():
                    to_up(source, k).start()
            to_pair(source, z - k).start()

        @pl.when(z + k <= chips - 1)
        def _():
            source = block(z + k, core)
            remote(source, source, down_send.at[k], down_recv.at[k], {"sp": sp, "dp": partner}).wait_recv()
            if k < chips - 1:
                @pl.when(z > 0)
                def _():
                    to_down(source, k).start()
            to_pair(source, z + k).start()

    if chips > 1:
        relay_columns(1)
    if square:
        got_x.wait_recv()
        relay_x = remote(token_rows(x_side, 0), token_rows(x_side, 0),
                         x_send.at[4], x_recv.at[4], {"sp": y_side, "dp": dp})
        relay_x.start()
        got_y.wait_recv()
        relay_y = remote(token_rows(y_side, 1), token_rows(y_side, 1),
                         x_send.at[5], x_recv.at[5], {"sp": x_side, "dp": dp})
        relay_y.start()
        token_sends += [relay_x, relay_y]
    for k in range(2, chips):
        relay_columns(k)

    for owner_z in range(chips):
        source = block(owner_z, 1 - core)
        remote(source, source, pair_send.at[owner_z], pair_recv.at[owner_z],
               {"sp": sp, "dp": partner}).wait_recv()
    if square:
        for owner, half, slot in (
            (x_side, 1, 1), (y_side, 0, 2), (corner, 0, 4), (corner, 1, 5)
        ):
            target = token_rows(owner, half)
            remote(target, target, x_send.at[slot], x_recv.at[slot],
                   {"sp": x_side, "dp": dp}).wait_recv()
    else:
        for i in range(parts - 1):
            target = token_rows(lax.rem(sp + parts - 1 - i, parts))
            remote(target, target, x_send.at[i], x_recv.at[i],
                   {"sp": greeted[0], "dp": dp}).wait_recv()
    for copy in token_sends:
        copy.wait_send()
    for owner_z in range(chips):
        to_pair(stage, owner_z).wait_send()
    for k in range(chips - 1):
        @pl.when(jnp.logical_and(z < chips - 1, z >= k))
        def _():
            to_up(stage, k).wait_send()

        @pl.when(jnp.logical_and(z > 0, z + k <= chips - 1))
        def _():
            to_down(stage, k).wait_send()
    own_rows.wait()
    own_cols.wait()


def gather(sequence, query_weight, key_weight, value_matrix, parts, chips, q_width, kv_width, first_kv_of):
    depth, width = query_weight.shape[0], q_width + 2 * kv_width
    row_count, features = sequence.shape
    dma = pltpu.SemaphoreType.DMA
    chain = dma((chips + 1,))
    return pl.pallas_call(
        functools.partial(gather_kernel, parts, chips, q_width, kv_width, first_kv_of),
        out_shape=(
            jax.ShapeDtypeStruct((parts * row_count, features), jnp.bfloat16),
            jax.ShapeDtypeStruct((chips * 2 * depth, width), jnp.bfloat16),
        ),
        in_specs=[pl.BlockSpec(memory_space=pltpu.VMEM), ANY, ANY, ANY],
        out_specs=(ANY, ANY),
        scratch_shapes=[
            pltpu.VMEM((depth, width), jnp.bfloat16),
            dma((max(6, parts),)), dma((max(6, parts),)), dma((2,)), dma((3,)),
            chain, chain, chain, chain, chain, chain,
        ],
        compiler_params=pltpu.CompilerParams(collective_id=0, has_side_effects=True),
        cost_estimate=pl.CostEstimate(flops=40_000_000_000, bytes_accessed=100_000_000, transcendentals=0),
        name="gather_rows_columns",
    )(sequence, query_weight, key_weight, value_matrix)


def exchange_kernel(parts, a_ref, o_ref, send, recv, own_sem):
    sp, dp = lax.axis_index("sp"), lax.axis_index("dp")
    row_count = o_ref.shape[1]
    barrier = pltpu.get_barrier_semaphore()
    peers = [lax.rem(sp + i, parts) for i in range(1, parts)]
    for peer in peers:
        pl.semaphore_signal(barrier, inc=1, device_id={"sp": peer, "dp": dp}, device_id_type=MESH)
    pl.semaphore_wait(barrier, parts - 1)
    copies = []
    for i, peer in enumerate(peers):
        copy = remote(a_ref.at[pl.ds(peer * row_count, row_count)], o_ref.at[sp],
                      send.at[i], recv.at[i], {"sp": peer, "dp": dp})
        copy.start()
        copies.append(copy)
    own = pltpu.make_async_copy(a_ref.at[pl.ds(sp * row_count, row_count)], o_ref.at[sp], own_sem)
    own.start()
    for i in range(parts - 1):
        target = o_ref.at[lax.rem(sp + parts - 1 - i, parts)]
        remote(target, target, send.at[i], recv.at[i], {"sp": peers[0], "dp": dp}).wait_recv()
    for copy in copies:
        copy.wait_send()
    own.wait()


def exchange(attended, parts):
    length, width = attended.shape
    row_count = length // parts
    dma = pltpu.SemaphoreType.DMA
    return pl.pallas_call(
        functools.partial(exchange_kernel, parts),
        out_shape=jax.ShapeDtypeStruct((parts, row_count, width), jnp.bfloat16),
        in_specs=[pl.BlockSpec(memory_space=pltpu.VMEM)],
        out_specs=ANY,
        scratch_shapes=[dma((parts,)), dma((parts,)), dma],
        compiler_params=pltpu.CompilerParams(collective_id=1, has_side_effects=True),
        cost_estimate=pl.CostEstimate(flops=10_000_000_000, bytes_accessed=20_000_000, transcendentals=0),
        name="exchange_heads",
    )(attended)


def project_kernel(q_heads, kv_heads, x_ref, g_ref, w_ref, qg_ref, kg_ref, cos_ref, sin_ref,
                   q_ref, k_ref, v_ref):
    x = x_ref[...].astype(jnp.float32)
    scale = lax.rsqrt(jnp.mean(x * x, axis=-1, keepdims=True) + EPS)
    normed = (x * scale * g_ref[...]).astype(jnp.bfloat16)
    mixed = jnp.dot(normed, w_ref[...], preferred_element_type=jnp.float32)
    cosine, sine = cos_ref[...], sin_ref[...]
    lane = lax.broadcasted_iota(jnp.int32, cosine.shape, 1)
    first = lane % (HEAD_WIDTH // 2) < HEAD_WIDTH // 4

    def finish(head, gain):
        head = head * lax.rsqrt(jnp.mean(head * head, axis=-1, keepdims=True) + EPS) * gain
        other = jnp.where(first, pltpu.roll(head, HEAD_WIDTH - HEAD_WIDTH // 4, 1),
                          pltpu.roll(head, HEAD_WIDTH // 4, 1))
        return (head * cosine + other * sine).astype(jnp.bfloat16)

    for h in range(q_heads):
        span = slice(h * HEAD_WIDTH, (h + 1) * HEAD_WIDTH)
        q_ref[:, span] = finish(mixed[:, span], qg_ref[...])
    for h in range(kv_heads):
        span = slice(h * HEAD_WIDTH, (h + 1) * HEAD_WIDTH)
        start = (q_heads + h) * HEAD_WIDTH
        k_ref[:, span] = finish(mixed[:, start:start + HEAD_WIDTH], kg_ref[...])
    v_ref[...] = mixed[:, (q_heads + kv_heads) * HEAD_WIDTH:].astype(jnp.bfloat16)


def project(rows, in_gain, columns, query_gain, key_gain, cosine, sine, q_heads, kv_heads, row_block):
    length, features = rows.shape
    width = columns.shape[1]
    q_width, kv_width = q_heads * HEAD_WIDTH, kv_heads * HEAD_WIDTH
    whole = lambda shape: pl.BlockSpec(shape, lambda i: (0, 0))
    part = lambda size: pl.BlockSpec((row_block, size), lambda i: (i, 0))
    return pl.pallas_call(
        functools.partial(project_kernel, q_heads, kv_heads),
        grid=(length // row_block,),
        out_shape=tuple(jax.ShapeDtypeStruct((length, n), jnp.bfloat16) for n in (q_width, kv_width, kv_width)),
        in_specs=[part(features), whole((1, features)), whole((features, width)),
                  whole((1, HEAD_WIDTH)), whole((1, HEAD_WIDTH)), part(HEAD_WIDTH), part(HEAD_WIDTH)],
        out_specs=(part(q_width), part(kv_width), part(kv_width)),
        cost_estimate=pl.CostEstimate(flops=2 * length * features * width, bytes_accessed=9_000_000, transcendentals=0),
        name="project_heads",
    )(rows, in_gain[None], columns, query_gain[None], key_gain[None], cosine, sine)


def attend_kernel(q_ref, k_ref, v_ref, o_ref):
    factor = HEAD_WIDTH ** (-0.5) * float(np.log2(np.e))
    scores = lax.dot_general(q_ref[...], k_ref[...], (((1,), (1,)), ((), ())),
                             preferred_element_type=jnp.float32)
    top = jnp.max(scores, axis=-1, keepdims=True)
    raised = jnp.exp2((scores - top) * factor)
    weights = (raised * (1.0 / jnp.sum(raised, axis=-1, keepdims=True))).astype(jnp.bfloat16)
    o_ref[...] = jnp.dot(weights, v_ref[...], preferred_element_type=jnp.float32).astype(jnp.bfloat16)


def attend(q, k, v, q_heads, kv_heads, row_block):
    length = q.shape[0]
    group = q_heads // kv_heads
    block = pl.BlockSpec((row_block, HEAD_WIDTH), lambda h, i: (i, h))
    keys = pl.BlockSpec((length, HEAD_WIDTH), lambda h, i: (0, h // group))
    return pl.pallas_call(
        attend_kernel,
        grid=(q_heads, length // row_block),
        out_shape=jax.ShapeDtypeStruct(q.shape, jnp.bfloat16),
        in_specs=[block, keys, keys],
        out_specs=block,
        cost_estimate=pl.CostEstimate(flops=4 * length * length * q_heads * HEAD_WIDTH,
                                      bytes_accessed=3_000_000, transcendentals=length * length * q_heads),
        name="attend_heads",
    )(q, k, v)


def output_kernel(a_ref, w_ref, g_ref, o_ref, total):
    step = pl.program_id(0)
    product = jnp.dot(a_ref[0], w_ref[...], preferred_element_type=jnp.float32)

    @pl.when(step == 0)
    def _():
        total[...] = product

    @pl.when(step > 0)
    def _():
        total[...] += product

    @pl.when(step == pl.num_programs(0) - 1)
    def _():
        x = total[...]
        scale = lax.rsqrt(jnp.mean(x * x, axis=-1, keepdims=True) + EPS)
        o_ref[...] = (x * scale * g_ref[...]).astype(jnp.bfloat16)


def output(returned, out_weight, out_gain):
    parts, row_count, width = returned.shape
    features = out_weight.shape[1]
    return pl.pallas_call(
        output_kernel,
        grid=(parts,),
        out_shape=jax.ShapeDtypeStruct((row_count, features), jnp.bfloat16),
        in_specs=[pl.BlockSpec((1, row_count, width), lambda s: (s, 0, 0)),
                  pl.BlockSpec((width, features), lambda s: (s, 0)),
                  pl.BlockSpec((1, features), lambda s: (0, 0))],
        out_specs=pl.BlockSpec((row_count, features), lambda s: (0, 0)),
        scratch_shapes=[pltpu.VMEM((row_count, features), jnp.float32)],
        cost_estimate=pl.CostEstimate(flops=2 * row_count * features * width * parts,
                                      bytes_accessed=10_000_000, transcendentals=0),
        name="output_rows",
    )(returned, out_weight, out_gain[None])


def rotation(length):
    quarter = HEAD_WIDTH // 4
    inverse_freq = (THETA ** (-np.arange(quarter, dtype=np.float32) / quarter)).astype(np.float32)

    def table(count):
        angle = (np.arange(count, dtype=np.float32)[:, None] * inverse_freq[None, :]).astype(np.float64)
        cosine, sine = np.cos(angle), np.sin(angle)
        return (np.concatenate([cosine, cosine], 1).astype(np.float32),
                np.concatenate([-sine, sine], 1).astype(np.float32))

    rows = -(-length // GRID_W)
    row_tables, col_tables = table(rows), table(GRID_W)
    half = HEAD_WIDTH // 2
    out = []
    for row, col in zip(row_tables, col_tables):
        row = jnp.broadcast_to(jnp.asarray(row)[:, None, :], (rows, GRID_W, half))
        col = jnp.broadcast_to(jnp.asarray(col)[None, :, :], (rows, GRID_W, half))
        out.append(jnp.concatenate([row, col], -1).reshape(rows * GRID_W, HEAD_WIDTH)[:length])
    return out


def on_device(parts, groups, tokens, in_gain, query_weight, key_weight, value_matrix,
              query_gain, key_gain, out_weight, out_gain):
    sequence = tokens[0]
    row_count = sequence.shape[0]
    q_heads = QUERY_HEAD_COUNT // parts
    kv_heads = max(1, KEY_VALUE_HEADS // parts)
    per_group = QUERY_HEAD_COUNT // KEY_VALUE_HEADS
    out_full = lax.all_gather(out_weight, "dp", axis=0, tiled=True)
    cosine, sine = rotation(parts * row_count)
    rows, columns = gather(
        sequence, query_weight, key_weight, value_matrix, parts, groups // 2,
        q_heads * HEAD_WIDTH, kv_heads * HEAD_WIDTH, lambda sp: sp * q_heads // per_group)
    q, k, v = project(rows, in_gain, columns, query_gain, key_gain, cosine, sine, q_heads, kv_heads, row_count)
    attended = attend(q, k, v, q_heads, kv_heads, row_count)
    returned = exchange(attended, parts)
    return output(returned, out_full, out_gain)[None]


def solution(mesh):
    placed = (P("dp", "sp", None), P(), P("dp", None), P("dp", None), P("dp", None),
              P(), P(), P("dp", None), P())
    return jax.shard_map(
        functools.partial(on_device, mesh.shape["sp"], mesh.shape["dp"]),
        mesh=mesh, in_specs=placed, out_specs=P("dp", "sp", None), check_vma=False,
    )
```

time: 198 us -> 167 us (0.84)
  Pallas kernels: 0 us -> 147 us
  waiting for transfers between devices: 76.6 us -> 0.73 us
  blocking collectives: 52.4 us -> 0 us
  other arithmetic: 21.4 us -> 2.01 us
  matrix products: 19 us -> 0 us
  local copies, waits for them, and re-layouts: 14.7 us -> 2.32 us
    pallas_call x0 -> x5, Pallas kernels: none -> 147 us  [the longest x1 99.4 us: gather(): pl.pallas_call(functools.partial(gather_kernel, parts, chips, q_width, kv...]
    all_gather x3 -> x1, waiting for transfers between devices: 75.9 us -> 0.02 us  [on_device(): out_full = lax.all_gather(out_weight, 'dp', axis=0, tiled=True)]
    all_gather x2 -> x0, blocking collectives: 35.8 us -> none  [the longest x1 19.1 us: on_device(): lax.all_gather(k_cols, 'dp', axis=0, tiled=True)]
    dot_general x6 -> x0, matrix products: 19 us -> none  [the longest x1 6.45 us: on_device(): blended = jnp.dot(shard_rows, joined, preferred_element_type=jnp.float32)]
    all_to_all x1 -> x0, blocking collectives: 16.7 us -> none  [on_device(): lax.all_to_all(attended, 'sp', split_axis=0, concat_axis=1, tiled=True)]
    reduce_sum x5 -> x0, other arithmetic: 6.98 us -> none  [the longest x2 3.57 us: one_block(): jnp.sum(raised, axis=-1, keepdims=True)]
    cos x1 -> x0, other arithmetic: 5.36 us -> none  [turn_half(): cosine = jnp.cos(angle)[:, None, :]]
    reshape x2 -> x0, local copies, waits for them, and re-layouts: 3.87 us -> none  [the longest x1 1.93 us: attend(): value_heads = local_v.reshape(length, key_value_slice, HEAD_WIDTH)]
  transfers between devices with their start and end apart: 3 -> 1, of which waited for: 2 -> 0; matrix products, arithmetic and copies ran while one was open for 22% -> 3% of each run, Pallas kernels for 0% -> 84%
where the time goes in v1:
time: 167 us; the launch traced here: 166 us
  Pallas kernels  147 us (88%)
  between operations  13.4 us (8%)
  local copies, waits for them, and re-layouts  2.32 us (1%)
  other arithmetic  2.01 us (1%)
    pallas_call x1, Pallas kernels, gather(): pl.pallas_call(functools.partial(gather_kernel, parts, chips, q_width, kv...  99.4 us
    pallas_call x1, Pallas kernels, exchange(): pl.pallas_call(functools.partial(exchange_kernel, parts), out_shape=jax.S...  16.3 us
    pallas_call x1, Pallas kernels, attend(): pl.pallas_call(attend_kernel, grid=(q_heads, length // row_block), out_sh...  14.8 us
    pallas_call x1, Pallas kernels, project(): pl.pallas_call(functools.partial(project_kernel, q_heads, kv_heads), grid...  9.37 us
    pallas_call x1, Pallas kernels, output(): pl.pallas_call(output_kernel, grid=(parts,), out_shape=jax.ShapeDtypeStru...  7.5 us
  transfers between devices with their start and end apart: 1, of which 0 were waited for; matrix products, arithmetic and copies ran while one was open for 3% of the time, Pallas kernels for 84%

profile of v1, /device:TPU:0, one launch (start us, length us, event | category | flops | bytes accessed | tf_op | source)
XLA Modules:
  0.0 166.0 jit_solution(1615345751835714608)
XLA Ops:
  6.5 0.0 copy-start
  6.5 0.0 all-gather.2.cloned.1.call-start
  6.5 0.7 all-gather.2.cloned.1.call-update
  7.3 0.7 broadcast_in_dim.42
  8.0 0.8 broadcast_in_dim.43
  8.8 1.0 pad_maximum_fusion
  9.8 0.7 broadcast_in_dim.44
  10.5 0.0 copy-done
  10.6 1.0 pad_maximum_fusion.1
  11.6 99.4 %gather_rows_columns.1 = (bf16[1024,2048]{1,0:T(8,128)(2,1)}, bf16[2048,768]{1,0:T(8,128)(2,1)}) custom-call(bf16[256,2048]{1,0:T(8,128)(2,1)} %bitcast.11, bf16[256,2048]{1,0:T(8,128)(2,1)} %wq_ref.1, bf16[256,512]{1,0:T(8,128)(2,1)} %wk_ref.1, bf16[256,512]{1,0:T(8,128)(2,1)} %wv_ref.1), custom_call_target="tpu_custom_call" | custom-call | flops 40000000000 | bytes 100000000 | tf_op jit(solution)/shard_map/gather_rows_columns/pallas_call | solution.py:212
  111.0 9.4 %project_heads.1 = (bf16[1024,512]{1,0:T(8,128)(2,1)}, bf16[1024,128]{1,0:T(8,128)(2,1)}, bf16[1024,128]{1,0:T(8,128)(2,1)}) custom-call(bf16[1024,2048]{1,0:T(8,128)(2,1)} %get-tuple-element.10.x_ref, f32[1,2048]{1,0:T(1,128)} %bitcast.12, bf16[2048,768]{1,0:T(8,128)(2,1)} %get-tuple-element.11.w_ref, f32[1,128]{1,0:T(1,128)} %bitcast.13, ...), custom_call_target="tpu_custom_call" | custom-call | flops 3221225472 | bytes 9000000 | tf_op jit(solution)/shard_map/project_heads/pallas_call | solution.py:303
  120.4 14.8 %attend_heads.1.a_ref = bf16[1024,512]{1,0:T(8,128)(2,1)} custom-call(bf16[1024,512]{1,0:T(8,128)(2,1)} %get-tuple-element.12.q_ref, bf16[1024,128]{1,0:T(8,128)(2,1)} %get-tuple-element.13.k_ref, bf16[1024,128]{1,0:T(8,128)(2,1)} %get-tuple-element.14.v_ref), custom_call_target="tpu_custom_call" | custom-call | flops 2147483648 | bytes 3000000 | tf_op jit(solution)/shard_map/attend_heads/pallas_call | solution.py:330
  135.3 16.3 %exchange_heads.1.a_ref = bf16[4,256,512]{2,1,0:T(8,128)(2,1)} custom-call(bf16[1024,512]{1,0:T(8,128)(2,1)} %attend_heads.1.a_ref), custom_call_target="tpu_custom_call" | custom-call | flops 10000000000 | bytes 20000000 | tf_op jit(solution)/shard_map/exchange_heads/pallas_call | solution.py:259
  151.6 0.0 all-gather.2.cloned.1.call-done.w_ref
  151.6 7.5 %output_rows.1 = bf16[256,2048]{1,0:T(8,128)(2,1)} custom-call(bf16[4,256,512]{2,1,0:T(8,128)(2,1)} %exchange_heads.1.a_ref, bf16[2048,2048]{1,0:T(8,128)(2,1)} %all-gather.2.cloned.1.call-done.w_ref, f32[1,2048]{1,0:T(1,128)} %bitcast.10), custom_call_target="tpu_custom_call" | custom-call | flops 2147483648 | bytes 10000000 | tf_op jit(solution)/shard_map/output_rows/pallas_call | solution.py:364
  (1 shorter events, 0.0 us)
Async XLA Ops:
  6.5 4.0 %copy-start = (f32[64,64]{1,0:T(8,128)S(1)}, f32[64,64]{1,0:T(8,128)}, u32[]{:S(2)}) copy-start(f32[64,64]{1,0:T(8,128)} %constant.11.clone) | copy-start | bytes 49156
  6.5 145.1 %all-gather.2.cloned.1.call-start = ((), (), s32[]{:S(2)}) async-start(), calls=%async_computation | async-start | bytes 9437184 | tf_op jit(solution)/shard_map/all_gather | solution.py:407
Sparse Core Ops, SparseCore 0:
  8.9 103.4 all-gather.1

commit v2 on v1

--- a/solution.py
+++ b/solution.py
@@ -27,7 +27,7 @@
 
 def gather_kernel(
     parts, chips, q_width, kv_width, first_kv_of,
-    x_ref, wq_ref, wk_ref, wv_ref, rows_ref, cols_ref,
+    x_ref, wq_ref, wk_ref, wv_ref, wo_ref, rows_ref, cols_ref, head_ref, tail_ref,
     stage, x_send, x_recv, own_sem, stage_sem,
     up_send, up_recv, down_send, down_recv, pair_send, pair_recv,
 ):
@@ -99,36 +99,47 @@
             token_sends.append(copy)
     own_rows = pltpu.make_async_copy(x_ref, token_rows(sp), own_sem.at[0])
     own_rows.start()
+    split = head_ref.shape[1]
+    out_head = wo_ref.at[:, pl.ds(0, split)]
+    own_tail = pltpu.make_async_copy(
+        wo_ref.at[:, pl.ds(split, tail_ref.shape[1])], tail_ref, own_sem.at[2])
+    own_tail.start()
 
     for load in loads:
         load.wait()
 
-    def block(owner_z, owner_core):
-        return cols_ref.at[pl.ds((owner_z * 2 + owner_core) * depth, depth)]
-
-    def to_up(src, k):
-        return remote(src, block(z - k, core), up_send.at[k], up_recv.at[k + 1],
+    gathered = (cols_ref, head_ref)
+    sources = (stage, out_head)
+
+    def block(t, owner_z, owner_core):
+        return gathered[t].at[pl.ds((owner_z * 2 + owner_core) * depth, depth)]
+
+    def to_up(t, src, k):
+        return remote(src, block(t, z - k, core), up_send.at[t, k], up_recv.at[t, k + 1],
                       {"sp": sp, "dp": dp + 2})
 
-    def to_down(src, k):
-        return remote(src, block(z + k, core), down_send.at[k], down_recv.at[k + 1],
+    def to_down(t, src, k):
+        return remote(src, block(t, z + k, core), down_send.at[t, k], down_recv.at[t, k + 1],
                       {"sp": sp, "dp": dp - 2})
 
-    def to_pair(src, owner_z):
-        return remote(src, block(owner_z, core), pair_send.at[owner_z], pair_recv.at[owner_z],
-                      {"sp": sp, "dp": partner})
-
-    @pl.when(z < chips - 1)
-    def _():
-        to_up(stage, 0).start()
-
-    @pl.when(z > 0)
-    def _():
-        to_down(stage, 0).start()
-
-    to_pair(stage, z).start()
-    own_cols = pltpu.make_async_copy(stage, block(z, core), own_sem.at[1])
-    own_cols.start()
+    def to_pair(t, src, owner_z):
+        return remote(src, block(t, owner_z, core), pair_send.at[t, owner_z],
+                      pair_recv.at[t, owner_z], {"sp": sp, "dp": partner})
+
+    own_copies = []
+    for t in range(2):
+        @pl.when(z < chips - 1)
+        def _():
+            to_up(t, sources[t], 0).start()
+
+        @pl.when(z > 0)
+        def _():
+            to_down(t, sources[t], 0).start()
+
+        to_pair(t, sources[t], z).start()
+        own = pltpu.make_async_copy(sources[t], block(t, z, core), own_sem.at[(1, 3)[t]])
+        own.start()
+        own_copies.append(own)
 
     if square:
         got_x = remote(x_ref.at[pl.ds(0, row_count // 2)], token_rows(x_side, 0),
@@ -136,29 +147,31 @@
         got_y = remote(x_ref.at[pl.ds(0, row_count // 2)], token_rows(y_side, 1),
                        x_send.at[3], x_recv.at[3], {"sp": y_side, "dp": dp})
 
-    def relay_columns(k):
+    def relay_columns(t, k):
         @pl.when(z >= k)
         def _():
-            source = block(z - k, core)
-            remote(source, source, up_send.at[k], up_recv.at[k], {"sp": sp, "dp": partner}).wait_recv()
+            source = block(t, z - k, core)
+            remote(source, source, up_send.at[t, k], up_recv.at[t, k],
+                   {"sp": sp, "dp": partner}).wait_recv()
             if k < chips - 1:
                 @pl.when(z < chips - 1)
                 def _():
-                    to_up(source, k).start()
-            to_pair(source, z - k).start()
+                    to_up(t, source, k).start()
+            to_pair(t, source, z - k).start()
 
         @pl.when(z + k <= chips - 1)
         def _():
-            source = block(z + k, core)
-            remote(source, source, down_send.at[k], down_recv.at[k], {"sp": sp, "dp": partner}).wait_recv()
+            source = block(t, z + k, core)
+            remote(source, source, down_send.at[t, k], down_recv.at[t, k],
+                   {"sp": sp, "dp": partner}).wait_recv()
             if k < chips - 1:
                 @pl.when(z > 0)
                 def _():
-                    to_down(source, k).start()
-            to_pair(source, z + k).start()
+                    to_down(t, source, k).start()
+            to_pair(t, source, z + k).start()
 
     if chips > 1:
-        relay_columns(1)
+        relay_columns(0, 1)
     if square:
         got_x.wait_recv()
         relay_x = remote(token_rows(x_side, 0), token_rows(x_side, 0),
@@ -169,13 +182,16 @@
                          x_send.at[5], x_recv.at[5], {"sp": x_side, "dp": dp})
         relay_y.start()
         token_sends += [relay_x, relay_y]
-    for k in range(2, chips):
-        relay_columns(k)
-
-    for owner_z in range(chips):
-        source = block(owner_z, 1 - core)
-        remote(source, source, pair_send.at[owner_z], pair_recv.at[owner_z],
-               {"sp": sp, "dp": partner}).wait_recv()
+    for k in range(1, chips):
+        if k > 1:
+            relay_columns(0, k)
+        relay_columns(1, k)
+
+    for t in range(2):
+        for owner_z in range(chips):
+            source = block(t, owner_z, 1 - core)
+            remote(source, source, pair_send.at[t, owner_z], pair_recv.at[t, owner_z],
+                   {"sp": sp, "dp": partner}).wait_recv()
     if square:
         for owner, half, slot in (
             (x_side, 1, 1), (y_side, 0, 2), (corner, 0, 4), (corner, 1, 5)
@@ -190,42 +206,49 @@
                    {"sp": greeted[0], "dp": dp}).wait_recv()
     for copy in token_sends:
         copy.wait_send()
-    for owner_z in range(chips):
-        to_pair(stage, owner_z).wait_send()
-    for k in range(chips - 1):
-        @pl.when(jnp.logical_and(z < chips - 1, z >= k))
-        def _():
-            to_up(stage, k).wait_send()
-
-        @pl.when(jnp.logical_and(z > 0, z + k <= chips - 1))
-        def _():
-            to_down(stage, k).wait_send()
+    for t in range(2):
+        for owner_z in range(chips):
+            to_pair(t, sources[t], owner_z).wait_send()
+        for k in range(chips - 1):
+            @pl.when(jnp.logical_and(z < chips - 1, z >= k))
+            def _():
+                to_up(t, sources[t], k).wait_send()
+
+            @pl.when(jnp.logical_and(z > 0, z + k <= chips - 1))
+            def _():
+                to_down(t, sources[t], k).wait_send()
     own_rows.wait()
-    own_cols.wait()
-
-
-def gather(sequence, query_weight, key_weight, value_matrix, parts, chips, q_width, kv_width, first_kv_of):
+    own_tail.wait()
+    for own in own_copies:
+        own.wait()
+
+
+def gather(sequence, query_weight, key_weight, value_matrix, out_weight, parts, chips, q_width, kv_width, first_kv_of):
     depth, width = query_weight.shape[0], q_width + 2 * kv_width
     row_count, features = sequence.shape
     dma = pltpu.SemaphoreType.DMA
-    chain = dma((chips + 1,))
+    chain = dma((2, chips + 1))
+    split = out_weight.shape[1] // 2
     return pl.pallas_call(
         functools.partial(gather_kernel, parts, chips, q_width, kv_width, first_kv_of),
         out_shape=(
             jax.ShapeDtypeStruct((parts * row_count, features), jnp.bfloat16),
             jax.ShapeDtypeStruct((chips * 2 * depth, width), jnp.bfloat16),
+            jax.ShapeDtypeStruct((chips * 2 * depth, split), jnp.bfloat16),
+            jax.ShapeDtypeStruct((depth, out_weight.shape[1] - split), jnp.bfloat16),
         ),
-        in_specs=[pl.BlockSpec(memory_space=pltpu.VMEM), ANY, ANY, ANY],
-        out_specs=(ANY, ANY),
+        in_specs=[pl.BlockSpec(memory_space=pltpu.VMEM), ANY, ANY, ANY,
+                  pl.BlockSpec(memory_space=pltpu.VMEM)],
+        out_specs=(ANY, ANY, ANY, ANY),
         scratch_shapes=[
             pltpu.VMEM((depth, width), jnp.bfloat16),
-            dma((max(6, parts),)), dma((max(6, parts),)), dma((2,)), dma((3,)),
+            dma((max(6, parts),)), dma((max(6, parts),)), dma((4,)), dma((3,)),
             chain, chain, chain, chain, chain, chain,
         ],
         compiler_params=pltpu.CompilerParams(collective_id=0, has_side_effects=True),
         cost_estimate=pl.CostEstimate(flops=40_000_000_000, bytes_accessed=100_000_000, transcendentals=0),
         name="gather_rows_columns",
-    )(sequence, query_weight, key_weight, value_matrix)
+    )(sequence, query_weight, key_weight, value_matrix, out_weight)
 
 
 def exchange_kernel(parts, a_ref, o_ref, send, recv, own_sem):
@@ -312,24 +335,27 @@
     )(rows, in_gain[None], columns, query_gain[None], key_gain[None], cosine, sine)
 
 
-def attend_kernel(q_ref, k_ref, v_ref, o_ref):
+def attend_kernel(group, q_ref, k_ref, v_ref, o_ref):
     factor = HEAD_WIDTH ** (-0.5) * float(np.log2(np.e))
-    scores = lax.dot_general(q_ref[...], k_ref[...], (((1,), (1,)), ((), ())),
-                             preferred_element_type=jnp.float32)
-    top = jnp.max(scores, axis=-1, keepdims=True)
-    raised = jnp.exp2((scores - top) * factor)
-    weights = (raised * (1.0 / jnp.sum(raised, axis=-1, keepdims=True))).astype(jnp.bfloat16)
-    o_ref[...] = jnp.dot(weights, v_ref[...], preferred_element_type=jnp.float32).astype(jnp.bfloat16)
+    for h in range(q_ref.shape[1] // HEAD_WIDTH):
+        span = slice(h * HEAD_WIDTH, (h + 1) * HEAD_WIDTH)
+        shared = slice(h // group * HEAD_WIDTH, (h // group + 1) * HEAD_WIDTH)
+        scores = lax.dot_general(q_ref[:, span], k_ref[:, shared], (((1,), (1,)), ((), ())),
+                                 preferred_element_type=jnp.float32)
+        top = jnp.max(scores, axis=-1, keepdims=True)
+        raised = jnp.exp2((scores - top) * factor)
+        weights = (raised * (1.0 / jnp.sum(raised, axis=-1, keepdims=True))).astype(jnp.bfloat16)
+        o_ref[:, span] = jnp.dot(
+            weights, v_ref[:, shared], preferred_element_type=jnp.float32).astype(jnp.bfloat16)
 
 
 def attend(q, k, v, q_heads, kv_heads, row_block):
     length = q.shape[0]
-    group = q_heads // kv_heads
-    block = pl.BlockSpec((row_block, HEAD_WIDTH), lambda h, i: (i, h))
-    keys = pl.BlockSpec((length, HEAD_WIDTH), lambda h, i: (0, h // group))
+    block = pl.BlockSpec((row_block, q.shape[1]), lambda i: (i, 0))
+    keys = pl.BlockSpec(k.shape, lambda i: (0, 0))
     return pl.pallas_call(
-        attend_kernel,
-        grid=(q_heads, length // row_block),
+        functools.partial(attend_kernel, q_heads // kv_heads),
+        grid=(length // row_block,),
         out_shape=jax.ShapeDtypeStruct(q.shape, jnp.bfloat16),
         in_specs=[block, keys, keys],
         out_specs=block,
@@ -339,17 +365,16 @@
     )(q, k, v)
 
 
-def output_kernel(a_ref, w_ref, g_ref, o_ref, total):
+def output_kernel(a_ref, head_ref, tail_ref, g_ref, o_ref, total):
     step = pl.program_id(0)
-    product = jnp.dot(a_ref[0], w_ref[...], preferred_element_type=jnp.float32)
+    split = head_ref.shape[1]
 
     @pl.when(step == 0)
     def _():
-        total[...] = product
-
-    @pl.when(step > 0)
-    def _():
-        total[...] += product
+        total[...] = jnp.zeros_like(total)
+
+    total[:, :split] += jnp.dot(a_ref[0], head_ref[...], preferred_element_type=jnp.float32)
+    total[:, split:] += jnp.dot(a_ref[0], tail_ref[...], preferred_element_type=jnp.float32)
 
     @pl.when(step == pl.num_programs(0) - 1)
     def _():
@@ -358,22 +383,24 @@
         o_ref[...] = (x * scale * g_ref[...]).astype(jnp.bfloat16)
 
 
-def output(returned, out_weight, out_gain):
+def output(returned, out_head, out_tail, out_gain):
     parts, row_count, width = returned.shape
-    features = out_weight.shape[1]
+    features = out_gain.shape[0]
+    split = out_head.shape[1]
     return pl.pallas_call(
         output_kernel,
         grid=(parts,),
         out_shape=jax.ShapeDtypeStruct((row_count, features), jnp.bfloat16),
         in_specs=[pl.BlockSpec((1, row_count, width), lambda s: (s, 0, 0)),
-                  pl.BlockSpec((width, features), lambda s: (s, 0)),
+                  pl.BlockSpec((width, split), lambda s: (s, 0)),
+                  pl.BlockSpec((width, features - split), lambda s: (s, 0)),
                   pl.BlockSpec((1, features), lambda s: (0, 0))],
         out_specs=pl.BlockSpec((row_count, features), lambda s: (0, 0)),
         scratch_shapes=[pltpu.VMEM((row_count, features), jnp.float32)],
         cost_estimate=pl.CostEstimate(flops=2 * row_count * features * width * parts,
                                       bytes_accessed=10_000_000, transcendentals=0),
         name="output_rows",
-    )(returned, out_weight, out_gain[None])
+    )(returned, out_head, out_tail, out_gain[None])
 
 
 def rotation(length):
@@ -391,9 +418,10 @@
     half = HEAD_WIDTH // 2
     out = []
     for row, col in zip(row_tables, col_tables):
-        row = jnp.broadcast_to(jnp.asarray(row)[:, None, :], (rows, GRID_W, half))
-        col = jnp.broadcast_to(jnp.asarray(col)[None, :, :], (rows, GRID_W, half))
-        out.append(jnp.concatenate([row, col], -1).reshape(rows * GRID_W, HEAD_WIDTH)[:length])
+        row = np.broadcast_to(row[:, None, :], (rows, GRID_W, half))
+        col = np.broadcast_to(col[None, :, :], (rows, GRID_W, half))
+        full = np.concatenate([row, col], -1).reshape(rows * GRID_W, HEAD_WIDTH)
+        out.append(jnp.asarray(full[:length]))
     return out
 
 
@@ -404,15 +432,15 @@
     q_heads = QUERY_HEAD_COUNT // parts
     kv_heads = max(1, KEY_VALUE_HEADS // parts)
     per_group = QUERY_HEAD_COUNT // KEY_VALUE_HEADS
-    out_full = lax.all_gather(out_weight, "dp", axis=0, tiled=True)
     cosine, sine = rotation(parts * row_count)
-    rows, columns = gather(
-        sequence, query_weight, key_weight, value_matrix, parts, groups // 2,
+    rows, columns, out_head, own_tail = gather(
+        sequence, query_weight, key_weight, value_matrix, out_weight, parts, groups // 2,
         q_heads * HEAD_WIDTH, kv_heads * HEAD_WIDTH, lambda sp: sp * q_heads // per_group)
+    out_tail = lax.all_gather(own_tail, "dp", axis=0, tiled=True)
     q, k, v = project(rows, in_gain, columns, query_gain, key_gain, cosine, sine, q_heads, kv_heads, row_count)
     attended = attend(q, k, v, q_heads, kv_heads, row_count)
     returned = exchange(attended, parts)
-    return output(returned, out_full, out_gain)[None]
+    return output(returned, out_head, out_tail, out_gain)[None]
 
 
 def solution(mesh):

time: 167 us -> 136 us (0.81)
  Pallas kernels: 147 us -> 114 us
  waiting for transfers between devices: 0.73 us -> 8.98 us
  local copies, waits for them, and re-layouts: 2.32 us -> 0 us
  other arithmetic: 2.01 us -> 0 us
    pallas_call x1, Pallas kernels: 99.4 us -> 68.3 us  [gather(): pl.pallas_call(functools.partial(gather_kernel, parts, chips, q_width, kv...]
    all_gather x1, waiting for transfers between devices: 0.02 us -> 8.97 us  [on_device(): out_tail = lax.all_gather(own_tail, 'dp', axis=0, tiled=True)]
    pallas_call x1, Pallas kernels: 14.8 us -> 12.2 us  [attend(): pl.pallas_call(functools.partial(attend_kernel, q_heads // kv_heads), gri...]
    broadcast_in_dim x4 -> x0, local copies, waits for them, and re-layouts: 2.31 us -> none  [the longest x2 1.47 us: rotation(): row = jnp.broadcast_to(jnp.asarray(row)[:, None, :], (rows, GRID_W, half))]
    concatenate x2 -> x0, other arithmetic: 2.01 us -> none  [rotation(): jnp.concatenate([row, col], -1).reshape(rows * GRID_W, HEAD_WIDTH)[:length]]
  transfers between devices with their start and end apart: 1 -> 1, of which waited for: 0 -> 1; matrix products, arithmetic and copies ran while one was open for 3% -> 0% of each run, Pallas kernels for 84% -> 28%
where the time goes in v2:
time: 136 us
  Pallas kernels  114 us (84%)
  between operations  13.4 us (10%)
  waiting for transfers between devices  8.98 us (7%)
    pallas_call x1, Pallas kernels, gather(): pl.pallas_call(functools.partial(gather_kernel, parts, chips, q_width, kv...  68.3 us
    pallas_call x1, Pallas kernels, exchange(): pl.pallas_call(functools.partial(exchange_kernel, parts), out_shape=jax.S...  16.7 us
    pallas_call x1, Pallas kernels, attend(): pl.pallas_call(functools.partial(attend_kernel, q_heads // kv_heads), gri...  12.2 us
    pallas_call x1, Pallas kernels, project(): pl.pallas_call(functools.partial(project_kernel, q_heads, kv_heads), grid...  9.34 us
    all_gather x1, waiting for transfers between devices, on_device(): out_tail = lax.all_gather(own_tail, 'dp', axis=0, tiled=True)  8.97 us
    pallas_call x1, Pallas kernels, output(): pl.pallas_call(output_kernel, grid=(parts,), out_shape=jax.ShapeDtypeStru...  7.13 us
  transfers between devices with their start and end apart: 1, of which 1 were waited for; matrix products, arithmetic and copies ran while one was open for 0% of the time, Pallas kernels for 28%

profile of v2, /device:TPU:0, one launch (start us, length us, event | category | flops | bytes accessed | tf_op | source)
XLA Modules:
  0.0 136.0 jit_solution(14631116492616686319)
XLA Ops:
  6.5 0.0 all-gather.2.cloned.1.call-start
  6.5 68.3 %gather_rows_columns.1 = (bf16[1024,2048]{1,0:T(8,128)(2,1)}, bf16[2048,768]{1,0:T(8,128)(2,1)}, bf16[2048,1024]{1,0:T(8,128)(2,1)}, bf16[256,1024]{1,0:T(8,128)(2,1)}) custom-call(bf16[256,2048]{1,0:T(8,128)(2,1)} %bitcast.7, bf16[256,2048]{1,0:T(8,128)(2,1)} %wq_ref.1, bf16[256,512]{1,0:T(8,128)(2,1)} %wk_ref.1, bf16[256,512]{1,0:T(8,128)(2,1)} %wv_ref.1, ...), custom_call_target="tpu_custom_call" | custom-call | flops 40000000000 | bytes 100000000 | tf_op jit(solution)/shard_map/gather_rows_columns/pallas_call | solution.py:232
  74.8 0.0 all-gather.2.cloned.1.call-update
  74.8 9.3 %project_heads.1 = (bf16[1024,512]{1,0:T(8,128)(2,1)}, bf16[1024,128]{1,0:T(8,128)(2,1)}, bf16[1024,128]{1,0:T(8,128)(2,1)}) custom-call(bf16[1024,2048]{1,0:T(8,128)(2,1)} %get-tuple-element.12.x_ref, f32[1,2048]{1,0:T(1,128)} %bitcast.8, bf16[2048,768]{1,0:T(8,128)(2,1)} %get-tuple-element.13.w_ref, f32[1,128]{1,0:T(1,128)} %bitcast.9, f32[1,128]{1,0:T(1,128)} %bitcast.10, ...), custom_call_target="tpu_custom_call" | custom-call | flops 3221225472 | bytes 9000000 | tf_op jit(solution)/shard_map/project_heads/pallas_call | solution.py:326
  84.2 12.2 %attend_heads.1.a_ref = bf16[1024,512]{1,0:T(8,128)(2,1)} custom-call(bf16[1024,512]{1,0:T(8,128)(2,1)} %get-tuple-element.14.q_ref, bf16[1024,128]{1,0:T(8,128)(2,1)} %get-tuple-element.15.k_ref, bf16[1024,128]{1,0:T(8,128)(2,1)} %get-tuple-element.16.v_ref), custom_call_target="tpu_custom_call" | custom-call | flops 2147483648 | bytes 3000000 | tf_op jit(solution)/shard_map/attend_heads/pallas_call | solution.py:356
  96.4 16.7 %exchange_heads.1.a_ref = bf16[4,256,512]{2,1,0:T(8,128)(2,1)} custom-call(bf16[1024,512]{1,0:T(8,128)(2,1)} %attend_heads.1.a_ref), custom_call_target="tpu_custom_call" | custom-call | flops 10000000000 | bytes 20000000 | tf_op jit(solution)/shard_map/exchange_heads/pallas_call | solution.py:282
  113.1 9.0 %all-gather.2.cloned.1.call-done.tail_ref = bf16[2048,1024]{1,0:T(8,128)(2,1)} async-done(((bf16[256,1024]{1,0:T(8,128)(2,1)}), bf16[2048,1024]{1,0:T(8,128)(2,1)}) %all-gather.2.cloned.1.call-update) | async-done | bytes 4194320 | tf_op jit(solution)/shard_map/all_gather | solution.py:439
  122.0 7.1 %output_rows.1 = bf16[256,2048]{1,0:T(8,128)(2,1)} custom-call(bf16[4,256,512]{2,1,0:T(8,128)(2,1)} %exchange_heads.1.a_ref, bf16[2048,1024]{1,0:T(8,128)(2,1)} %get-tuple-element.17.head_ref, bf16[2048,1024]{1,0:T(8,128)(2,1)} %all-gather.2.cloned.1.call-done.tail_ref, f32[1,2048]{1,0:T(1,128)} %bitcast.6), custom_call_target="tpu_custom_call" | custom-call | flops 2147483648 | bytes 10000000 | tf_op jit(solution)/shard_map/output_rows/pallas_call | solution.py:390
Async XLA Ops:
  6.5 115.5 %all-gather.2.cloned.1.call-start = ((), (), s32[]{:S(2)}) async-start(), calls=%async_computation | async-start | bytes 4718592 | tf_op jit(solution)/shard_map/all_gather | solution.py:439
Sparse Core Ops, SparseCore 0:
  75.0 47.0 all-gather.1

commit v3 on v2

--- a/solution.py
+++ b/solution.py
@@ -228,7 +228,7 @@
     row_count, features = sequence.shape
     dma = pltpu.SemaphoreType.DMA
     chain = dma((2, chips + 1))
-    split = out_weight.shape[1] // 2
+    split = out_weight.shape[1] * 5 // 8
     return pl.pallas_call(
         functools.partial(gather_kernel, parts, chips, q_width, kv_width, first_kv_of),
         out_shape=(

time: 136 us -> 136 us (level)
  waiting for transfers between devices: 8.98 us -> 0.27 us
  Pallas kernels: 114 us -> 122 us
    all_gather x1, waiting for transfers between devices: 8.97 us -> 0.26 us  [on_device(): out_tail = lax.all_gather(own_tail, 'dp', axis=0, tiled=True)]
    pallas_call x1, Pallas kernels: 68.3 us -> 76.9 us  [gather(): pl.pallas_call(functools.partial(gather_kernel, parts, chips, q_width, kv...]
where the time goes in v3:
time: 136 us
  Pallas kernels  122 us (90%)
  between operations  13.4 us (10%)
    pallas_call x1, Pallas kernels, gather(): pl.pallas_call(functools.partial(gather_kernel, parts, chips, q_width, kv...  76.9 us
    pallas_call x1, Pallas kernels, exchange(): pl.pallas_call(functools.partial(exchange_kernel, parts), out_shape=jax.S...  16.7 us
    pallas_call x1, Pallas kernels, attend(): pl.pallas_call(functools.partial(attend_kernel, q_heads // kv_heads), gri...  12.2 us
    pallas_call x1, Pallas kernels, project(): pl.pallas_call(functools.partial(project_kernel, q_heads, kv_heads), grid...  9.35 us
    pallas_call x1, Pallas kernels, output(): pl.pallas_call(output_kernel, grid=(parts,), out_shape=jax.ShapeDtypeStru...  7.19 us
  transfers between devices with their start and end apart: 1, of which 1 were waited for; matrix products, arithmetic and copies ran while one was open for 0% of the time, Pallas kernels for 28%

profile of v3, /device:TPU:0, one launch (start us, length us, event | category | flops | bytes accessed | tf_op | source)
XLA Modules:
  0.0 136.0 jit_solution(2952197599275814488)
XLA Ops:
  6.5 0.0 all-gather.2.cloned.1.call-start
  6.5 76.9 %gather_rows_columns.1 = (bf16[1024,2048]{1,0:T(8,128)(2,1)}, bf16[2048,768]{1,0:T(8,128)(2,1)}, bf16[2048,1280]{1,0:T(8,128)(2,1)}, bf16[256,768]{1,0:T(8,128)(2,1)}) custom-call(bf16[256,2048]{1,0:T(8,128)(2,1)} %bitcast.7, bf16[256,2048]{1,0:T(8,128)(2,1)} %wq_ref.1, bf16[256,512]{1,0:T(8,128)(2,1)} %wk_ref.1, bf16[256,512]{1,0:T(8,128)(2,1)} %wv_ref.1, ...), custom_call_target="tpu_custom_call" | custom-call | flops 40000000000 | bytes 100000000 | tf_op jit(solution)/shard_map/gather_rows_columns/pallas_call | solution.py:232
  83.4 0.0 all-gather.2.cloned.1.call-update
  83.5 9.3 %project_heads.1 = (bf16[1024,512]{1,0:T(8,128)(2,1)}, bf16[1024,128]{1,0:T(8,128)(2,1)}, bf16[1024,128]{1,0:T(8,128)(2,1)}) custom-call(bf16[1024,2048]{1,0:T(8,128)(2,1)} %get-tuple-element.12.x_ref, f32[1,2048]{1,0:T(1,128)} %bitcast.8, bf16[2048,768]{1,0:T(8,128)(2,1)} %get-tuple-element.13.w_ref, f32[1,128]{1,0:T(1,128)} %bitcast.9, f32[1,128]{1,0:T(1,128)} %bitcast.10, ...), custom_call_target="tpu_custom_call" | custom-call | flops 3221225472 | bytes 9000000 | tf_op jit(solution)/shard_map/project_heads/pallas_call | solution.py:326
  92.8 12.2 %attend_heads.1.a_ref = bf16[1024,512]{1,0:T(8,128)(2,1)} custom-call(bf16[1024,512]{1,0:T(8,128)(2,1)} %get-tuple-element.14.q_ref, bf16[1024,128]{1,0:T(8,128)(2,1)} %get-tuple-element.15.k_ref, bf16[1024,128]{1,0:T(8,128)(2,1)} %get-tuple-element.16.v_ref), custom_call_target="tpu_custom_call" | custom-call | flops 2147483648 | bytes 3000000 | tf_op jit(solution)/shard_map/attend_heads/pallas_call | solution.py:356
  105.0 16.7 %exchange_heads.1.a_ref = bf16[4,256,512]{2,1,0:T(8,128)(2,1)} custom-call(bf16[1024,512]{1,0:T(8,128)(2,1)} %attend_heads.1.a_ref), custom_call_target="tpu_custom_call" | custom-call | flops 10000000000 | bytes 20000000 | tf_op jit(solution)/shard_map/exchange_heads/pallas_call | solution.py:282
  121.7 0.3 all-gather.2.cloned.1.call-done.tail_ref
  122.0 7.2 %output_rows.1 = bf16[256,2048]{1,0:T(8,128)(2,1)} custom-call(bf16[4,256,512]{2,1,0:T(8,128)(2,1)} %exchange_heads.1.a_ref, bf16[2048,1280]{1,0:T(8,128)(2,1)} %get-tuple-element.17.head_ref, bf16[2048,768]{1,0:T(8,128)(2,1)} %all-gather.2.cloned.1.call-done.tail_ref, f32[1,2048]{1,0:T(1,128)} %bitcast.6), custom_call_target="tpu_custom_call" | custom-call | flops 2147483648 | bytes 10000000 | tf_op jit(solution)/shard_map/output_rows/pallas_call | solution.py:390
Async XLA Ops:
  6.5 115.5 %all-gather.2.cloned.1.call-start = ((), (), s32[]{:S(2)}) async-start(), calls=%async_computation | async-start | bytes 3538944 | tf_op jit(solution)/shard_map/all_gather | solution.py:439
Sparse Core Ops, SparseCore 0:
  83.6 38.3 all-gather.1
